TPU v7x, 32 devices: a whole 2x2x4 slice. The times are simulated.
32 devices in a mesh: rep: 4 (over z), fs: 4 (over y, x), tp: 2 (over core).
Axes of the slice: x: 2, y: 2, z: 4, core: 2. Of those that a mesh axis runs over, the one named last changes fastest.
Arguments:
- tokens_in: bfloat16 [3072, 1024], P(('rep', 'fs', 'tp')), may hold values from -6 to 6
- out_grad: bfloat16 [3072, 1024], P(('rep', 'fs', 'tp')), may hold values from -6 to 6
- gate_weight: bfloat16 [1024, 2816], P('fs', 'tp'), may hold values from -0.1875 to 0.1875
- up_weight: bfloat16 [1024, 2816], P('fs', 'tp'), may hold values from -0.1875 to 0.1875
- down_weight: bfloat16 [2816, 1024], P('tp', 'fs'), may hold values from -0.109375 to 0.109375
Outputs:
- grad_in: bfloat16 [3072, 1024], P(('rep', 'fs', 'tp'))
- grad_gate_w: float32 [1024, 2816], P('fs', 'tp')
- grad_up_w: float32 [1024, 2816], P('fs', 'tp')
- grad_down_w: float32 [2816, 1024], P('tp', 'fs')
All inputs are finite; a program needn't handle non-finite values.
Results may differ from a plain program's by a relative error of at most 0.02.
Values may be sent and summed in bfloat16 or wider, within the bound.
A program may use at most 64 MiB of HBM per device.

v0:
```python
import jax
import jax.numpy as jnp
from jax import lax
from jax.sharding import PartitionSpec as P


def summed_rows(product, width, axis):
    everything = product(jnp.int32(0), lax.axis_size(axis) * width)
    own = lax.psum_scatter(everything.astype(jnp.bfloat16), axis, scatter_dimension=0, tiled=True)
    return own.astype(jnp.float32)


def regroup(block, outer, inner, dimension):
    old_shape = block.shape
    width = old_shape[dimension] // (outer * inner)
    new_shape = old_shape[:dimension] + (outer, inner, width) + old_shape[dimension + 1 :]
    layout = list(range(len(new_shape)))
    layout[dimension] = dimension + 1
    layout[dimension + 1] = dimension
    return jnp.transpose(block.reshape(new_shape), layout).reshape(old_shape)


def contract_last(left, right):
    return lax.dot_general(
        left, right, (((1,), (1,)), ((), ())), preferred_element_type=jnp.float32
    )


def contract_first(left, right):
    return lax.dot_general(
        left, right, (((0,), (0,)), ((), ())), preferred_element_type=jnp.float32
    )


def body(tokens_in, out_grad, gate_weight, up_weight, down_weight):
    replicas = lax.axis_size("rep")
    shards = lax.axis_size("fs")
    columns = lax.axis_size("tp")
    local_rows = tokens_in.shape[0]
    model_width = gate_weight.shape[0] * shards
    hidden_cols = gate_weight.shape[1]
    factor = (local_rows * replicas * shards * columns) ** (-0.5)
    part_rows = gate_weight.shape[0] // replicas
    offset = lax.axis_index("rep") * part_rows
    pieces = (
        lax.dynamic_slice_in_dim(gate_weight, offset, part_rows, 0),
        lax.dynamic_slice_in_dim(up_weight, offset, part_rows, 0),
        lax.dynamic_slice_in_dim(down_weight, offset, part_rows, 1),
    )
    gate_full, up_full, down_full = (
        lax.all_gather(pieces[0], ("rep", "fs"), axis=0, tiled=True),
        lax.all_gather(pieces[1], ("rep", "fs"), axis=0, tiled=True),
        lax.all_gather(pieces[2], ("rep", "fs"), axis=1, tiled=True),
    )
    gate_full = regroup(gate_full, replicas, shards, 0)
    up_full = regroup(up_full, replicas, shards, 0)
    down_full = regroup(down_full, replicas, shards, 1)
    tokens_all, grads_all = (
        lax.all_gather(tokens_in, "tp", axis=0, tiled=True),
        lax.all_gather(out_grad, "tp", axis=0, tiled=True),
    )
    gate = jnp.dot(tokens_all, gate_full, preferred_element_type=jnp.float32).astype(jnp.bfloat16)
    up_proj = jnp.dot(tokens_all, up_full, preferred_element_type=jnp.float32).astype(jnp.bfloat16)
    gate_wide = gate.astype(jnp.float32)
    up_wide = up_proj.astype(jnp.float32)
    sigmoid = jax.nn.sigmoid(gate_wide)
    activated = gate_wide * sigmoid
    hidden = (activated * up_wide).astype(jnp.bfloat16)
    grad_hidden = contract_last(grads_all, down_full).astype(jnp.bfloat16)
    grad_wide = grad_hidden.astype(jnp.float32)
    grad_gate = (grad_wide * up_wide * sigmoid * (1.0 + gate_wide * (1.0 - sigmoid))).astype(
        jnp.bfloat16
    )
    grad_up = (grad_wide * activated).astype(jnp.bfloat16)

    def input_term(start, count):
        gate_rows = lax.dynamic_slice_in_dim(grad_gate, start, count, 0)
        up_rows = lax.dynamic_slice_in_dim(grad_up, start, count, 0)
        return contract_last(gate_rows, gate_full) + contract_last(up_rows, up_full)

    grad_in = summed_rows(input_term, local_rows, "tp").astype(jnp.bfloat16)

    def weight_term(token_order, grad_order):

        def term(start, count):
            token_cols = lax.dynamic_slice_in_dim(token_order, start, count, 1)
            grad_cols = lax.dynamic_slice_in_dim(grad_order, start, count, 1)
            return factor * jnp.concatenate(
                [
                    contract_first(token_cols, grad_gate),
                    contract_first(token_cols, grad_up),
                    contract_first(grad_cols, hidden),
                ],
                axis=1,
            )

        return term

    owned = summed_rows(weight_term(tokens_all, grads_all), model_width // shards, "fs")
    summed = lax.psum(owned.astype(jnp.bfloat16), "rep").astype(jnp.float32)
    grad_gate_w = summed[:, :hidden_cols]
    grad_up_w = summed[:, hidden_cols : 2 * hidden_cols]
    grad_down_w = summed[:, 2 * hidden_cols :].T
    return (grad_in, grad_gate_w, grad_up_w, grad_down_w)


def solution(mesh):
    placed = (
        P(("rep", "fs", "tp"), None),
        P(("rep", "fs", "tp"), None),
        P("fs", "tp"),
        P("fs", "tp"),
        P("tp", "fs"),
    )
    return jax.shard_map(
        body,
        mesh=mesh,
        in_specs=placed,
        out_specs=(P(("rep", "fs", "tp"), None), P("fs", "tp"), P("fs", "tp"), P("tp", "fs")),
        check_vma=False,
    )
```

profile of v0, /device:TPU:0, one launch (start us, length us, event | category | flops | bytes accessed | tf_op | source)
XLA Modules:
  0.0 423.7 jit_solution(640800213981886636)
XLA Ops:
  7.2 0.0 copy-start
  7.2 0.0 copy-start.9
  7.2 0.0 copy-start.10
  7.2 0.0 all-gather.8.cloned.1.call-start
  7.3 1.0 copy-done
  8.3 0.7 constant_dynamic-slice_fusion
  9.0 0.0 all-gather.8.cloned.1.call-update
  9.0 0.0 all-gather.6.cloned.1.call-start
  9.0 1.6 constant_dynamic-slice_fusion.1
  10.7 0.0 all-gather.6.cloned.1.call-update
  10.7 0.0 all-gather.4.cloned.1.call-start
  10.7 1.2 constant_dynamic-slice_fusion.2
  11.9 0.8 copy.21
  12.7 0.0 all-gather.4.cloned.1.call-update
  12.7 0.0 reduce-scatter.5.cloned.1.call-start
  12.8 0.0 copy-done.9
  12.8 2.2 all_gather.18
  15.0 0.0 copy-done.10
  15.0 2.2 all_gather.16
  17.2 62.8 %all-gather.8.cloned.1.call-done = bf16[1024,1408]{1,0:T(8,128)(2,1)} async-done(((bf16[64,1408]{1,0:T(8,128)(2,1)}), bf16[1024,1408]{1,0:T(8,128)(2,1)}) %all-gather.8.cloned.1.call-update) | async-done | bytes 2883600 | tf_op jit(solution)/shard_map/all_gather | solution.py:51
  80.1 2.1 copy.18
  82.1 65.9 %all-gather.6.cloned.1.call-done = bf16[1024,1408]{1,0:T(8,128)(2,1)} async-done(((bf16[64,1408]{1,0:T(8,128)(2,1)}), bf16[1024,1408]{1,0:T(8,128)(2,1)}) %all-gather.6.cloned.1.call-update) | async-done | bytes 2883600 | tf_op jit(solution)/shard_map/all_gather | solution.py:52
  148.1 3.7 copy.17
  151.7 64.4 %all-gather.4.cloned.1.call-done = bf16[1408,1024]{0,1:T(8,128)(2,1)} async-done(((bf16[1408,64]{0,1:T(8,128)(2,1)}), bf16[1408,1024]{0,1:T(8,128)(2,1)}) %all-gather.4.cloned.1.call-update) | async-done | bytes 2883600 | tf_op jit(solution)/shard_map/all_gather | solution.py:53
  216.1 0.0 copy-start.2
  216.1 2.2 copy.16
  218.3 0.5 copy-done.2
  218.8 0.8 fusion.4
  219.6 0.0 copy-start.8
  219.6 0.8 fusion.2
  220.4 0.2 copy-done.8
  220.6 1.0 convolution_bitcast_fusion
  221.5 0.9 multiply_convert_fusion.1
  222.4 0.0 copy-start.5
  222.5 0.0 copy-start.7
  222.5 0.9 convolution_bitcast_fusion.1
  223.4 0.0 copy-done.5
  223.4 0.0 copy-done.7
  223.4 1.0 convolution_bitcast_fusion.2
  224.4 5.1 %fusion = bf16[1024,4224]{0,1:T(8,128)(2,1)} fusion(f32[1024,1408]{0,1:T(8,128)S(1)} %convolution_bitcast_fusion, f32[1024,1408]{0,1:T(8,128)S(1)} %convolution_bitcast_fusion.1, f32[1024,1408]{0,1:T(8,128)S(1)} %convolution_bitcast_fusion.2), kind=kLoop, calls=%fused_computation.1 | loop fusion | flops 17301504 | bytes 25952256 | tf_op jit(solution)/shard_map/convert_element_type | solution.py:9
  229.5 0.0 reduce-scatter.5.cloned.1.call-update
  229.5 0.0 all-reduce.2.cloned.1.call-start
  229.6 87.2 %reduce-scatter.5.cloned.1.call-done = bf16[256,4224]{0,1:T(8,128)(2,1)} async-done(((bf16[1024,4224]{0,1:T(8,128)(2,1)}), bf16[256,4224]{0,1:T(8,128)(2,1)}) %reduce-scatter.5.cloned.1.call-update) | async-done | bytes 2162704 | tf_op jit(solution)/shard_map/reduce_scatter | solution.py:9
  316.8 0.0 all-reduce.2.cloned.1.call-update
  316.8 0.0 copy-start.6
  316.8 0.0 reduce-scatter.3.cloned.1.call-start
  316.9 0.0 copy-start.3
  316.9 2.3 fusion.12
  319.2 0.0 copy-done.6
  319.2 0.0 copy-done.3
  319.2 1.9 fusion.7
  321.1 0.0 reduce-scatter.3.cloned.1.call-update
  321.1 86.2 %all-reduce.2.cloned.1.call-done = bf16[256,4224]{0,1:T(8,128)(2,1)} async-done(((bf16[256,4224]{0,1:T(8,128)(2,1)}), bf16[256,4224]{0,1:T(8,128)(2,1)}) %all-reduce.2.cloned.1.call-update) | async-done | bytes 2162704 | tf_op jit(solution)/shard_map/psum | solution.py:100
  407.3 2.6 fusion.11
  410.0 1.5 copy.20
  411.5 0.0 copy-start.4
  411.5 3.0 copy.19
  414.6 0.0 copy-done.4
  414.6 0.0 copy-start.1
  414.6 0.3 convert_element_type.66
  414.9 1.2 slice_bitcast_fusion
  416.1 0.8 reduce-scatter.3.cloned.1.call-done
  416.9 0.0 copy-done.1
Async XLA Ops:
  7.2 1.1 copy-start
  7.2 5.6 %copy-start.9 = (bf16[96,1024]{1,0:T(8,128)(2,1)S(1)}, bf16[96,1024]{1,0:T(8,128)(2,1)}, u32[]{:S(2)}) copy-start(bf16[96,1024]{1,0:T(8,128)(2,1)} %param.5) | copy-start | bytes 589828
  7.2 7.8 %copy-start.10 = (bf16[96,1024]{1,0:T(8,128)(2,1)S(1)}, bf16[96,1024]{1,0:T(8,128)(2,1)}, u32[]{:S(2)}) copy-start(bf16[96,1024]{1,0:T(8,128)(2,1)} %param.6) | copy-start | bytes 589828
  7.2 72.9 %all-gather.8.cloned.1.call-start = ((), (), s32[]{:S(2)}) async-start(), calls=%async_computation.4 | async-start | bytes 3063808 | tf_op jit(solution)/shard_map/all_gather | solution.py:51
  9.0 139.1 %all-gather.6.cloned.1.call-start = ((), (), s32[]{:S(2)}) async-start(), calls=%async_computation.3 | async-start | bytes 3063808 | tf_op jit(solution)/shard_map/all_gather | solution.py:52
  10.7 205.4 %all-gather.4.cloned.1.call-start = ((), (), s32[]{:S(2)}) async-start(), calls=%async_computation.2 | async-start | bytes 3063808 | tf_op jit(solution)/shard_map/all_gather | solution.py:53
  12.7 304.0 %reduce-scatter.5.cloned.1.call-start = ((), (), s32[]{:S(2)}) async-start(), calls=%async_computation.6 | async-start | bytes 10813440 | tf_op jit(solution)/shard_map/reduce_scatter | solution.py:9
  216.1 2.7 copy-start.2
  219.6 1.0 copy-start.8
  222.4 1.0 copy-start.5
  222.5 1.0 copy-start.7
  229.5 177.8 %all-reduce.2.cloned.1.call-start = ((), (), s32[]{:S(2)}) async-start(), calls=%async_computation.7 | async-start | bytes 4325376 | tf_op jit(solution)/shard_map/psum | solution.py:100
  316.8 2.4 copy-start.6
  316.8 100.0 %reduce-scatter.3.cloned.1.call-start = ((), (), s32[]{:S(2)}) async-start(), calls=%async_computation.5 | async-start | bytes 589824 | tf_op jit(solution)/shard_map/reduce_scatter | solution.py:9
  316.9 2.3 copy-start.3
  411.5 3.1 copy-start.4
  414.6 2.3 copy-start.1
Sparse Core Ops, SparseCore 0:
  11.3 68.6 all-gather.7
  83.4 64.6 all-gather.5
  151.4 64.6 all-gather.3
  229.6 87.1 reduce-scatter.4
  319.0 88.2 all-reduce.1
  410.0 6.8 reduce-scatter.2
where the time goes:
time: 424 us
  waiting for transfers between devices  367 us (87%)
  local copies, waits for them, and re-layouts  22.4 us (5%)
  between operations  14.3 us (3%)
  matrix products  9.5 us (2%)
  other arithmetic  5.43 us (1%)
  blocking collectives  4.42 us (1%)
    reduce_scatter x2, waiting for transfers between devices, summed_rows(): lax.psum_scatter(everything.astype(jnp.bfloat16), axis, scatter_dimension...  88 us
    psum x1, waiting for transfers between devices, body(): summed = lax.psum(owned.astype(jnp.bfloat16), 'rep').astype(jnp.float32)  86.2 us
    all_gather x1, waiting for transfers between devices, body(): lax.all_gather(pieces[1], ('rep', 'fs'), axis=0, tiled=True)  65.9 us
    all_gather x1, waiting for transfers between devices, body(): lax.all_gather(pieces[2], ('rep', 'fs'), axis=1, tiled=True)  64.4 us
    all_gather x1, waiting for transfers between devices, body(): lax.all_gather(pieces[0], ('rep', 'fs'), axis=0, tiled=True)  62.8 us
  transfers between devices with their start and end apart: 6, of which 6 were waited for; matrix products, arithmetic and copies ran while one was open for 5% of the time, Pallas kernels for 0%

commit v1 on v0

--- a/solution.py
+++ b/solution.py
@@ -97,7 +97,7 @@
         return term
 
     owned = summed_rows(weight_term(tokens_all, grads_all), model_width // shards, "fs")
-    summed = lax.psum(owned.astype(jnp.bfloat16), "rep").astype(jnp.float32)
+    summed = jnp.sum(lax.all_gather(owned.astype(jnp.bfloat16), "rep"), axis=0).astype(jnp.float32)
     grad_gate_w = summed[:, :hidden_cols]
     grad_up_w = summed[:, hidden_cols : 2 * hidden_cols]
     grad_down_w = summed[:, 2 * hidden_cols :].T

time: 424 us -> 530 us (1.25)
  waiting for transfers between devices: 367 us -> 429 us
  other arithmetic: 5.43 us -> 29.2 us
  local copies, waits for them, and re-layouts: 22.4 us -> 42.1 us
    all_gather x0 -> x1, waiting for transfers between devices: none -> 150 us  [body(): lax.all_gather(owned.astype(jnp.bfloat16), 'rep')]
    psum x1 -> x0, waiting for transfers between devices: 86.2 us -> none  [body(): summed = lax.psum(owned.astype(jnp.bfloat16), 'rep').astype(jnp.float32)]
    reduce_sum x0 -> x1, other arithmetic: none -> 21.8 us  [body(): jnp.sum(lax.all_gather(owned.astype(jnp.bfloat16), 'rep'), axis=0)]
    all_gather x0 -> x1, local copies, waits for them, and re-layouts: none -> 16.7 us  [body(): lax.all_gather(owned.astype(jnp.bfloat16), 'rep')]
  transfers between devices with their start and end apart: 6 -> 6, of which waited for: 6 -> 5; matrix products, arithmetic and copies ran while one was open for 5% -> 12% of each run, Pallas kernels for 0% -> 0%
where the time goes in v1:
time: 530 us; the launch traced here: 529 us
  waiting for transfers between devices  429 us (81%)
  local copies, waits for them, and re-layouts  42.1 us (8%)
  other arithmetic  29.2 us (6%)
  between operations  14.2 us (3%)
  matrix products  10.4 us (2%)
    all_gather x1, waiting for transfers between devices, body(): lax.all_gather(owned.astype(jnp.bfloat16), 'rep')  150 us
    reduce_scatter x2, waiting for transfers between devices, summed_rows(): lax.psum_scatter(everything.astype(jnp.bfloat16), axis, scatter_dimension...  87.2 us
    all_gather x1, waiting for transfers between devices, body(): lax.all_gather(pieces[1], ('rep', 'fs'), axis=0, tiled=True)  64.3 us
    all_gather x1, waiting for transfers between devices, body(): lax.all_gather(pieces[2], ('rep', 'fs'), axis=1, tiled=True)  64.3 us
    all_gather x1, waiting for transfers between devices, body(): lax.all_gather(pieces[0], ('rep', 'fs'), axis=0, tiled=True)  63 us
    reduce_sum x1, other arithmetic, body(): jnp.sum(lax.all_gather(owned.astype(jnp.bfloat16), 'rep'), axis=0)  21.8 us
    all_gather x1, local copies, waits for them, and re-layouts, body(): lax.all_gather(owned.astype(jnp.bfloat16), 'rep')  16.7 us
  transfers between devices with their start and end apart: 6, of which 5 were waited for; matrix products, arithmetic and copies ran while one was open for 12% of the time, Pallas kernels for 0%

profile of v1, /device:TPU:0, one launch (start us, length us, event | category | flops | bytes accessed | tf_op | source)
XLA Modules:
  0.0 529.1 jit_solution(489253781435811890)
XLA Ops:
  7.2 0.0 copy-start
  7.2 0.0 copy-start.6
  7.2 0.0 copy-start.7
  7.2 0.0 all-gather.10.cloned.1.call-start
  7.3 1.0 copy-done
  8.3 0.7 constant_dynamic-slice_fusion
  9.0 0.0 all-gather.10.cloned.1.call-update
  9.0 0.0 all-gather.8.cloned.1.call-start
  9.0 1.6 constant_dynamic-slice_fusion.1
  10.7 0.0 all-gather.8.cloned.1.call-update
  10.7 0.0 all-gather.6.cloned.1.call-start
  10.7 1.2 constant_dynamic-slice_fusion.2
  11.9 0.8 copy.21
  12.7 0.0 all-gather.6.cloned.1.call-update
  12.7 0.0 reduce-scatter.5.cloned.1.call-start
  12.8 0.0 copy-done.6
  12.8 2.2 all_gather.24
  15.0 0.0 copy-done.7
  15.0 2.1 all_gather.22
  17.1 63.0 %all-gather.10.cloned.1.call-done = bf16[1024,1408]{1,0:T(8,128)(2,1)} async-done(((bf16[64,1408]{1,0:T(8,128)(2,1)}), bf16[1024,1408]{1,0:T(8,128)(2,1)}) %all-gather.10.cloned.1.call-update) | async-done | bytes 2883600 | tf_op jit(solution)/shard_map/all_gather | solution.py:51
  80.1 3.7 copy.18
  83.7 64.3 %all-gather.8.cloned.1.call-done = bf16[1024,1408]{1,0:T(8,128)(2,1)} async-done(((bf16[64,1408]{1,0:T(8,128)(2,1)}), bf16[1024,1408]{1,0:T(8,128)(2,1)}) %all-gather.8.cloned.1.call-update) | async-done | bytes 2883600 | tf_op jit(solution)/shard_map/all_gather | solution.py:52
  148.1 3.7 copy.17
  151.8 64.3 %all-gather.6.cloned.1.call-done = bf16[1408,1024]{0,1:T(8,128)(2,1)} async-done(((bf16[1408,64]{0,1:T(8,128)(2,1)}), bf16[1408,1024]{0,1:T(8,128)(2,1)}) %all-gather.6.cloned.1.call-update) | async-done | bytes 2883600 | tf_op jit(solution)/shard_map/all_gather | solution.py:53
  216.1 0.0 copy-start.3
  216.1 2.2 copy.16
  218.3 0.5 copy-done.3
  218.8 0.0 copy-start.2
  218.8 0.8 fusion.4
  219.6 1.0 copy-done.2
  220.6 0.8 fusion.2
  221.4 1.0 convolution_bitcast_fusion
  222.4 1.0 multiply_convert_fusion.1
  223.4 1.0 convolution_bitcast_fusion.1
  224.3 0.9 convolution_bitcast_fusion.2
  225.3 5.1 fusion
  230.4 0.0 reduce-scatter.5.cloned.1.call-update
  230.4 0.0 all-gather.12.cloned.1.call-start
  230.4 87.2 %reduce-scatter.5.cloned.1.call-done = bf16[256,4224]{0,1:T(8,128)(2,1)} async-done(((bf16[1024,4224]{0,1:T(8,128)(2,1)}), bf16[256,4224]{0,1:T(8,128)(2,1)}) %reduce-scatter.5.cloned.1.call-update) | async-done | bytes 2162704 | tf_op jit(solution)/shard_map/reduce_scatter | solution.py:9
  317.7 0.0 all-gather.12.cloned.1.call-update
  317.7 0.2 reduce-scatter.3.cloned.1.call-start
  317.9 0.0 copy-start.4
  317.9 3.1 fusion.12
  321.0 0.0 copy-done.4
  321.0 1.9 fusion.7
  322.9 0.0 reduce-scatter.3.cloned.1.call-update
  322.9 149.6 %all-gather.12.cloned.1.call-done = bf16[1024,4224]{0,1:T(8,128)(2,1)} async-done(((bf16[256,4224]{0,1:T(8,128)(2,1)}), bf16[1024,4224]{0,1:T(8,128)(2,1)}) %all-gather.12.cloned.1.call-update) | async-done | bytes 8650768 | tf_op jit(solution)/shard_map/all_gather | solution.py:100
  472.5 16.7 %reshape.32 = bf16[4,256,4224]{1,0,2:T(4,128)(2,1)} reshape(bf16[1024,4224]{0,1:T(8,128)(2,1)} %all-gather.12.cloned.1.call-done) | data formatting | bytes 17301504 | tf_op jit(solution)/shard_map/all_gather | solution.py:100
  489.2 21.8 %reduce_sum.12 = bf16[256,4224]{0,1:T(8,128)(2,1)S(1)} reduce(bf16[4,256,4224]{1,0,2:T(4,128)(2,1)} %reshape.32, bf16[]{:T(256)} %constant.17.clone.1), dimensions={0}, to_apply=%region_2.0 | reduce | flops 3244032 | bytes 10813442 | tf_op jit(solution)/shard_map/reduce_sum | solution.py:100
  511.0 1.8 fusion.11
  512.8 2.3 convert_element_type.68
  515.1 0.0 copy-start.5
  515.1 3.0 copy.20
  518.1 0.0 copy-done.5
  518.1 0.0 copy-start.1
  518.1 1.5 copy.19
  519.7 2.6 slice_bitcast_fusion
  522.2 0.0 reduce-scatter.3.cloned.1.call-done
  522.2 0.0 copy-done.1
Async XLA Ops:
  7.2 1.1 copy-start
  7.2 5.6 %copy-start.6 = (bf16[96,1024]{1,0:T(8,128)(2,1)S(1)}, bf16[96,1024]{1,0:T(8,128)(2,1)}, u32[]{:S(2)}) copy-start(bf16[96,1024]{1,0:T(8,128)(2,1)} %param.5) | copy-start | bytes 589828
  7.2 7.8 %copy-start.7 = (bf16[96,1024]{1,0:T(8,128)(2,1)S(1)}, bf16[96,1024]{1,0:T(8,128)(2,1)}, u32[]{:S(2)}) copy-start(bf16[96,1024]{1,0:T(8,128)(2,1)} %param.6) | copy-start | bytes 589828
  7.2 72.9 %all-gather.10.cloned.1.call-start = ((), (), s32[]{:S(2)}) async-start(), calls=%async_computation.4 | async-start | bytes 3063808 | tf_op jit(solution)/shard_map/all_gather | solution.py:51
  9.0 139.1 %all-gather.8.cloned.1.call-start = ((), (), s32[]{:S(2)}) async-start(), calls=%async_computation.3 | async-start | bytes 3063808 | tf_op jit(solution)/shard_map/all_gather | solution.py:52
  10.7 205.4 %all-gather.6.cloned.1.call-start = ((), (), s32[]{:S(2)}) async-start(), calls=%async_computation.2 | async-start | bytes 3063808 | tf_op jit(solution)/shard_map/all_gather | solution.py:53
  12.7 304.9 %reduce-scatter.5.cloned.1.call-start = ((), (), s32[]{:S(2)}) async-start(), calls=%async_computation.6 | async-start | bytes 10813440 | tf_op jit(solution)/shard_map/reduce_scatter | solution.py:9
  216.1 2.7 copy-start.3
  218.8 1.8 copy-start.2
  230.4 242.1 %all-gather.12.cloned.1.call-start = ((), (), s32[]{:S(2)}) async-start(), calls=%async_computation.7 | async-start | bytes 10813440 | tf_op jit(solution)/shard_map/all_gather | solution.py:100
  317.7 204.5 %reduce-scatter.3.cloned.1.call-start = ((), (), s32[]{:S(2)}) async-start(), calls=%async_computation.5 | async-start | bytes 589824 | tf_op jit(solution)/shard_map/reduce_scatter | solution.py:9
  317.9 3.1 copy-start.4
  515.1 3.0 copy-start.5
  518.1 4.1 copy-start.1
Sparse Core Ops, SparseCore 0:
  11.3 68.6 all-gather.9
  83.4 64.6 all-gather.7
  151.4 64.6 all-gather.5
  230.5 87.1 reduce-scatter.4
  319.1 153.3 all-gather.11
  475.2 6.0 reduce-scatter.2
